TPU v7x, 32 devices: a whole 2x2x4 slice. The times are simulated.
32 devices in a mesh: grp: 2 (over y), sp: 4 (over z), tp: 4 (over x, core).
Axes of the slice: x: 2, y: 2, z: 4, core: 2. Of those that a mesh axis runs over, the one named last changes fastest.
Arguments:
- queries: bfloat16 [2048, 1024], P(('grp', 'sp'), 'tp'), parts along dimension 0, may hold values from -7 to 10
- keys: bfloat16 [2048, 1024], P(('grp', 'sp'), 'tp'), parts along dimension 0, may hold values from -14 to 7
- values: bfloat16 [2048, 1024], P(('grp', 'sp'), 'tp'), parts along dimension 0, may hold values from -6 to 6
- resid: bfloat16 [2048, 2048], P(('grp', 'sp', 'tp')), parts along dimension 0, may hold values from -18 to 18
- out_weight: bfloat16 [1024, 2048], P('tp'), may hold values from -0.375 to 0.375
- gate_weight: bfloat16 [2048, 3072], P('sp', 'tp'), may hold values from -0.125 to 0.125
- value_weight: bfloat16 [2048, 3072], P('sp', 'tp'), may hold values from -0.125 to 0.125
- conv_gate: float32 [3, 3072], P(None, 'tp'), may hold values from -3 to 3
- conv_value: float32 [3, 3072], P(None, 'tp'), may hold values from -3 to 3
- norm_gain: float32 [2048], replicated, may hold values from 0.1 to 1.9
- down_weight: bfloat16 [3072, 2048], P('tp', 'sp'), may hold values from -0.109375 to 0.109375
Outputs:
- layer_out: bfloat16 [2048, 2048], P(('grp', 'sp', 'tp')), parts along dimension 0
There are 2 independent parts, one for each index of `grp`. A program takes and returns all parts, laid end to end along the dimension named above; an argument that names none is the same for every part. Nothing has to cross between parts.
All inputs are finite; a program needn't handle non-finite values.
Results may differ from a plain program's by a relative error of at most 0.0058.
Values may be sent and summed in bfloat16 or wider, within the bound.
A program may use at most 128 MiB of HBM per device.

v0:
```python
import jax
import jax.numpy as jnp
from jax import lax
from jax.sharding import PartitionSpec as P

HEAD = 64
epsilon = 1e-06


def shifted(block, axis, distance):
    devices = range(lax.axis_size(axis))
    route = [(i - distance, i) for i in devices if i - distance in devices]
    return lax.ppermute(block, axis, route)


def block_terms(query_rows, key_rows, value_rows, query_place, key_place):
    scores = jnp.einsum(
        "qhe,khe->hqk", query_rows, key_rows, preferred_element_type=jnp.float32
    ) * HEAD ** (-0.5)
    causal = (key_place[None, :] < query_place[:, None])[None]
    stay_log = jnp.where(causal, jax.nn.log_sigmoid(-scores), 0.0)
    suffix = lax.cumsum(stay_log, axis=2, reverse=True) - stay_log
    local_weight = jnp.where(causal, jnp.exp(jax.nn.log_sigmoid(scores) + suffix), 0.0).astype(
        jnp.bfloat16
    )
    part = jnp.einsum("hqk,khe->hqe", local_weight, value_rows, preferred_element_type=jnp.float32)
    return (jnp.sum(stay_log, axis=2), part)


def normalize(state, norm_gain):
    values = state.astype(jnp.float32)
    scaled = values * lax.rsqrt(jnp.mean(values * values, axis=-1, keepdims=True) + epsilon)
    return (scaled * norm_gain).astype(jnp.bfloat16)


def causal_conv(rim_rows, rows, taps):
    extended = jnp.concatenate([rim_rows, rows], axis=0).astype(jnp.float32)
    length = rows.shape[0]
    total = jnp.zeros(rows.shape, jnp.float32)
    for start_displacement in range(taps.shape[0]):
        total = (
            total
            + taps[start_displacement] * extended[start_displacement : start_displacement + length]
        )
    return total


def body(
    queries,
    keys,
    values,
    resid,
    out_weight,
    gate_weight,
    value_weight,
    conv_gate,
    conv_value,
    norm_gain,
    down_weight,
):
    tok_dev = queries.shape[0]
    mix_local = queries.shape[1]
    head_count = mix_local // HEAD
    sp_count = lax.axis_size("sp")
    block = tok_dev * min(sp_count, max(1, 1024 // tok_dev))
    paired = jnp.concatenate([keys, values], axis=1)
    gathered = lax.all_gather(paired, "sp", axis=0, tiled=True)
    mine = lax.axis_index("sp")
    query_place = mine * tok_dev + jnp.arange(tok_dev, dtype=jnp.int32)
    query_rows = queries.reshape(tok_dev, head_count, HEAD)

    def add_block(index, carry):
        start = index * block
        piece = lax.dynamic_slice_in_dim(gathered, start, block, 0)
        key_rows = piece[:, :mix_local].reshape(block, head_count, HEAD)
        value_rows = piece[:, mix_local:].reshape(block, head_count, HEAD)
        key_place = start + jnp.arange(block, dtype=jnp.int32)
        total, part = block_terms(query_rows, key_rows, value_rows, query_place, key_place)
        return carry * jnp.exp(total)[:, :, None] + part

    start_carry = jnp.zeros((head_count, tok_dev, HEAD), jnp.float32)
    attended = lax.fori_loop(0, mine * tok_dev // block + 1, add_block, start_carry)
    mixed = jnp.transpose(attended, (1, 0, 2)).reshape(tok_dev, mix_local).astype(jnp.bfloat16)
    projected = lax.psum_scatter(
        jnp.dot(mixed, out_weight, preferred_element_type=jnp.float32),
        "tp",
        scatter_dimension=0,
        tiled=True,
    )
    state = (resid.astype(jnp.float32) + projected).astype(jnp.bfloat16)
    normed = lax.all_gather(normalize(state, norm_gain), "tp", axis=0, tiled=True)
    ff_local = gate_weight.shape[1]
    gate_full = jnp.dot(
        normed,
        lax.all_gather(gate_weight, "sp", axis=0, tiled=True),
        preferred_element_type=jnp.float32,
    )
    value_full = jnp.dot(
        normed,
        lax.all_gather(value_weight, "sp", axis=0, tiled=True),
        preferred_element_type=jnp.float32,
    )
    gate_pre = gate_full.astype(jnp.bfloat16)
    value_pre = value_full.astype(jnp.bfloat16)
    taps_count = conv_gate.shape[0]
    rim = jnp.concatenate(
        [gate_pre[tok_dev - taps_count + 1 :], value_pre[tok_dev - taps_count + 1 :]], axis=1
    )
    before = shifted(rim, "sp", 1)
    conv_gate_out = causal_conv(before[:, :ff_local], gate_pre, conv_gate)
    conv_value_out = causal_conv(before[:, ff_local:], value_pre, conv_value)
    gated = (jax.nn.silu(conv_gate_out) * conv_value_out).astype(jnp.bfloat16)
    partial_sum = jnp.dot(
        gated,
        lax.all_gather(down_weight, "sp", axis=1, tiled=True),
        preferred_element_type=jnp.float32,
    )
    ffn_share = lax.psum_scatter(partial_sum, "tp", scatter_dimension=0, tiled=True)
    return (state.astype(jnp.float32) + ffn_share).astype(jnp.bfloat16)


def solution(mesh):
    placed = (
        P(("grp", "sp"), "tp"),
        P(("grp", "sp"), "tp"),
        P(("grp", "sp"), "tp"),
        P(("grp", "sp", "tp"), None),
        P("tp", None),
        P("sp", "tp"),
        P("sp", "tp"),
        P(None, "tp"),
        P(None, "tp"),
        P(),
        P("tp", "sp"),
    )
    return jax.shard_map(
        body, mesh=mesh, in_specs=placed, out_specs=P(("grp", "sp", "tp"), None), check_vma=False
    )
```

profile of v0, /device:TPU:0, one launch (start us, length us, event | category | flops | bytes accessed | tf_op | source)
XLA Modules:
  0.0 383.4 jit_solution(949477178948924257)
XLA Ops:
  6.5 1.1 copy.14
  7.6 1.0 copy.15
  8.6 0.7 pad_maximum_fusion
  9.4 0.0 all-gather.6.cloned.1.call-update
  9.4 0.0 reduce-scatter.3.cloned.1.call-start
  9.5 1.0 copy.16
  10.5 31.7 %all-gather.6.cloned.1.call-done = bf16[1024,512]{0,1:T(8,128)(2,1)} async-done(((bf16[256,512]{0,1:T(8,128)(2,1)}), bf16[1024,512]{0,1:T(8,128)(2,1)}) %all-gather.6.cloned.1.call-update) | async-done | bytes 1048592 | tf_op jit(solution)/shard_map/all_gather | solution.py:67
  42.2 56.0 %while.11 = (s32[]{:T(128)}, f32[4,256,64]{1,2,0:T(8,128)S(1)}, s32[]{:T(128)}, bf16[1024,512]{0,1:T(8,128)(2,1)}, bf16[256,4,64]{0,2,1:T(8,128)(2,1)S(1)}, /*index=5*/s32[]{:T(128)}, s32[]{:T(128)}, s32[]{:T(128)}, f32[]{:T(128)}) while((s32[]{:T(128)}, f32[4,256,64]{1,2,0:T(8,128)S(1)}, s32[]{:T(128)}, ...), condition=%wide.region_4.5_spmd.clone, body=%wide.region_0.4_spmd.clone.sunk | while | flops 447937792 | bytes 93714576 | solution.py:82
  42.2 1.3 fusion.66
  43.5 2.9 fusion.67
  46.4 0.2 broadcast_compare_fusion.2
  46.6 5.6 %fusion.68 = (f32[4,256]{1,0:T(4,128)S(1)}, f32[4,256,1024]{2,1,0:T(8,128)S(1)}) fusion(f32[4,256,1024]{2,1,0:T(8,128)} %get-tuple-element.134, u8[256,1024]{1,0:T(8,128)(4,1)S(1)} %get-tuple-element.135, pred[256,1024]{1,0:T(8,128)(4,1)S(1)} %broadcast_compare_fusion.2), kind=kLoop, calls=%fused_computation.20.clone.1 | loop fusion | flops 13630464 | bytes 8916992 | tf_op jit(solution)/shard_map/while/body/reduce_sum | solution.py:27
  52.3 3.0 copy.21
  55.2 5.5 %copy.22 = f32[4,256,8,128]{1,2,3,0:T(8,128)} copy(f32[4,256,8,128]{3,2,1,0:T(8,128)} %bitcast.44) | data formatting | bytes 8388608 | tf_op jit(solution)/shard_map/reshape
  60.8 10.8 %fusion.69 = f32[4,256,8,128]{1,2,3,0:T(8,128)S(1)} fusion(f32[4,256,8,128]{1,2,3,0:T(8,128)} %copy.22), kind=kOutput, calls=%fused_computation.65.clone.1 | output fusion | flops 133169152 | bytes 8388608 | tf_op jit(solution)/shard_map/reduce-window
  71.6 2.0 copy-done.1
  73.6 0.1 reduce-window.16
  73.6 4.5 %broadcast_add_fusion.2 = f32[4,256,8,128]{1,2,3,0:T(8,128)} fusion(f32[4,256,8,128]{1,2,3,0:T(8,128)} %copy-done.1, f32[4,256,8]{1,2,0:T(8,128)S(1)} %slice.148), kind=kLoop, calls=%fused_computation.10.clone.1 | loop fusion | flops 1048576 | bytes 8421376 | tf_op jit(solution)/shard_map/reduce_window_sum | solution.py:22
  78.1 5.5 %copy.23 = f32[4,256,8,128]{3,2,1,0:T(8,128)} copy(f32[4,256,8,128]{1,2,3,0:T(8,128)} %broadcast_add_fusion.2) | data formatting | bytes 8388608 | tf_op jit(solution)/shard_map/reduce_window_sum | solution.py:22
  83.6 4.9 %reduce_window_sum.20 = f32[4,256,1024]{2,1,0:T(8,128)} reshape(f32[4,256,8,128]{3,2,1,0:T(8,128)} %copy.23) | data formatting | bytes 8388608 | tf_op jit(solution)/shard_map/reduce_window_sum | solution.py:22
  88.5 9.5 %fusion.70 = f32[4,256,64]{1,2,0:T(8,128)S(1)} fusion(bf16[1024,4,64]{0,2,1:T(8,128)(2,1)S(1)} %bitcast.46, f32[4,256,1024]{2,1,0:T(8,128)} %reduce_window_sum.20, f32[4,256,1024]{2,1,0:T(8,128)} %get-tuple-element.134, pred[256,1024]{1,0:T(8,128)(4,1)S(1)} %broadcast_compare_fusion.2, f32[4,256,64]{1,2,0:T(8,128)S(1)} %get-tuple-element.148, ...), kind=kOutput, calls=%fused_computation.12.clone.1 | convolution fusion | flops 159514624 | bytes 9965568 | tf_op jit(solution)/shard_map/while/body/hqk,khe->hqe/dot_general | solution.py:26
  98.3 1.8 fusion.39
  100.1 0.0 reduce-scatter.3.cloned.1.call-update
  100.2 0.0 all-gather.10.cloned.1.call-start
  100.2 0.7 all-gather.10.cloned.1.call-update
  100.9 0.0 all-gather.8.cloned.1.call-start
  100.9 28.8 %reduce-scatter.3.cloned.1.call-done = f32[64,2048]{1,0:T(8,128)} async-done(((f32[256,2048]{1,0:T(8,128)}), f32[64,2048]{1,0:T(8,128)}) %reduce-scatter.3.cloned.1.call-update) | async-done | bytes 524304 | tf_op jit(solution)/shard_map/reduce_scatter | solution.py:84
  129.8 1.2 fusion.22
  131.0 0.8 fusion.24
  131.9 0.0 all-gather.8.cloned.1.call-update
  131.9 0.0 all-gather.12.cloned.1.call-start
  131.9 0.5 all-gather.12.cloned.1.call-update
  132.5 0.0 all-gather.14.cloned.1.call-start
  132.5 0.5 all-gather.14.cloned.1.call-update
  133.1 0.0 reduce-scatter.5.cloned.1.call-start
  133.1 61.7 %all-gather.10.cloned.1.call-done = bf16[2048,768]{1,0:T(8,128)(2,1)} async-done(((bf16[512,768]{1,0:T(8,128)(2,1)}), bf16[2048,768]{1,0:T(8,128)(2,1)}) %all-gather.10.cloned.1.call-update) | async-done | bytes 3145744 | tf_op jit(solution)/shard_map/all_gather | solution.py:95
  194.8 16.8 %all-gather.8.cloned.1.call-done = bf16[256,2048]{1,0:T(8,128)(2,1)} async-done(((bf16[64,2048]{1,0:T(8,128)(2,1)}), bf16[256,2048]{1,0:T(8,128)(2,1)}) %all-gather.8.cloned.1.call-update) | async-done | bytes 1048592 | tf_op jit(solution)/shard_map/all_gather | solution.py:91
  211.6 3.3 convolution_convert_fusion.1
  215.0 61.6 %all-gather.12.cloned.1.call-done = bf16[2048,768]{1,0:T(8,128)(2,1)} async-done(((bf16[512,768]{1,0:T(8,128)(2,1)}), bf16[2048,768]{1,0:T(8,128)(2,1)}) %all-gather.12.cloned.1.call-update) | async-done | bytes 3145744 | tf_op jit(solution)/shard_map/all_gather | solution.py:100
  276.5 2.9 convolution_convert_fusion
  279.4 1.3 collective-permute-start
  280.8 0.1 slice_reduce_fusion.2
  280.8 1.2 collective-permute-done
  282.1 0.2 maximum_convert_fusion
  282.2 57.8 %all-gather.14.cloned.1.call-done = bf16[768,2048]{1,0:T(8,128)(2,1)} async-done(((bf16[768,512]{1,0:T(8,128)(2,1)}), bf16[768,2048]{1,0:T(8,128)(2,1)}) %all-gather.14.cloned.1.call-update) | async-done | bytes 3145744 | tf_op jit(solution)/shard_map/all_gather | solution.py:115
  340.1 4.7 %fusion.26 = f32[256,2048]{1,0:T(8,128)} fusion(bf16[768,2048]{1,0:T(8,128)(2,1)} %all-gather.14.cloned.1.call-done, f32[258,768]{1,0:T(8,128)S(1)} %get-tuple-element.84, f32[258,768]{1,0:T(8,128)S(1)} %get-tuple-element.83, f32[768]{0:T(1024)S(1)} %get-tuple-element.59, f32[768]{0:T(1024)S(1)} %get-tuple-element.60, f32[768]{0:T(1024)S(1)} %get-tuple-element.58, ...), kind=kOutput, calls=%fused_computation.45 | convolution fusion | flops 808452096 | bytes 9986048 | tf_op jit(solution)/shard_map/dot_general | solution.py:113
  344.8 30.0 %reduce-scatter.5.cloned.1.call-done = f32[64,2048]{1,0:T(8,128)} async-done(((f32[256,2048]{1,0:T(8,128)}), f32[64,2048]{1,0:T(8,128)}) %reduce-scatter.5.cloned.1.call-update) | async-done | bytes 524304 | tf_op jit(solution)/shard_map/reduce_scatter | solution.py:118
  374.8 1.8 fusion.25
  (27 shorter events, 0.1 us)
Async XLA Ops:
  6.5 91.8 %copy-start = (bf16[256,2048]{1,0:T(8,128)(2,1)S(1)}, bf16[256,2048]{1,0:T(8,128)(2,1)}, u32[]{:S(2)}) copy-start(bf16[256,2048]{1,0:T(8,128)(2,1)} %param.17) | copy-start | bytes 3145732
  6.5 35.7 %all-gather.6.cloned.1.call-start = ((), (), s32[]{:S(2)}) async-start(), calls=%async_computation.2 | async-start | bytes 1310720 | tf_op jit(solution)/shard_map/all_gather | solution.py:67
  9.4 120.4 %reduce-scatter.3.cloned.1.call-start = ((), (), s32[]{:S(2)}) async-start(), calls=%async_computation.3 | async-start | bytes 2621440 | tf_op jit(solution)/shard_map/reduce_scatter | solution.py:84
  71.6 2.0 copy-start.1
  98.2 31.5 %copy-start.2 = (bf16[64,2048]{1,0:T(8,128)(2,1)S(1)}, bf16[64,2048]{1,0:T(8,128)(2,1)}, u32[]{:S(2)}) copy-start(bf16[64,2048]{1,0:T(8,128)(2,1)} %param.16) | copy-start | bytes 786436
  98.3 32.8 %copy-start.3 = (f32[2048]{0:T(1024)S(1)}, f32[2048]{0:T(1024)}, u32[]{:S(2)}) copy-start(f32[2048]{0:T(1024)} %param.22) | copy-start | bytes 24580
  100.2 94.7 %all-gather.10.cloned.1.call-start = ((), (), s32[]{:S(2)}) async-start(), calls=%async_computation.5 | async-start | bytes 3932160 | tf_op jit(solution)/shard_map/all_gather | solution.py:95
  100.9 110.7 %all-gather.8.cloned.1.call-start = ((), (), s32[]{:S(2)}) async-start(), calls=%async_computation.4 | async-start | bytes 1310720 | tf_op jit(solution)/shard_map/all_gather | solution.py:91
  131.9 144.6 %all-gather.12.cloned.1.call-start = ((), (), s32[]{:S(2)}) async-start(), calls=%async_computation.6 | async-start | bytes 3932160 | tf_op jit(solution)/shard_map/all_gather | solution.py:100
  132.5 207.6 %all-gather.14.cloned.1.call-start = ((), (), s32[]{:S(2)}) async-start(), calls=%async_computation.7 | async-start | bytes 3932160 | tf_op jit(solution)/shard_map/all_gather | solution.py:115
  133.1 241.7 %reduce-scatter.5.cloned.1.call-start = ((), (), s32[]{:S(2)}) async-start(), calls=%async_computation.8 | async-start | bytes 2621440 | tf_op jit(solution)/shard_map/reduce_scatter | solution.py:118
  211.6 64.9 %copy-start.6 = (bf16[256,2048]{1,0:T(8,128)(2,1)S(1)}, bf16[256,2048]{1,0:T(8,128)(2,1)}, u32[]{:S(2)}) copy-start(bf16[256,2048]{1,0:T(8,128)(2,1)} %all-gather.8.cloned.1.call-done) | copy-start | bytes 3145732
  214.9 65.8 %copy-start.4 = (f32[3,768]{1,0:T(4,128)S(1)}, f32[3,768]{1,0:T(4,128)}, u32[]{:S(2)}) copy-start(f32[3,768]{1,0:T(4,128)} %param.21) | copy-start | bytes 27652
  214.9 65.8 %copy-start.5 = (f32[3,768]{1,0:T(4,128)S(1)}, f32[3,768]{1,0:T(4,128)}, u32[]{:S(2)}) copy-start(f32[3,768]{1,0:T(4,128)} %param.20) | copy-start | bytes 27652
  279.4 2.6 collective-permute-start
Sparse Core Ops, SparseCore 0:
  9.5 32.6 all-gather.5
  100.3 29.4 reduce-scatter.2
  131.4 63.4 all-gather.9
  196.3 15.3 all-gather.7
  213.0 63.4 all-gather.11
  278.0 62.0 all-gather.13
  344.9 29.8 reduce-scatter.4
where the time goes:
time: 384 us; the launch traced here: 383 us
  waiting for transfers between devices  292 us (76%)
  other arithmetic  25.9 us (7%)
  local copies, waits for them, and re-layouts  25.4 us (7%)
  matrix products  25.1 us (7%)
  between operations  13.7 us (4%)
    all_gather x1, waiting for transfers between devices, body(): lax.all_gather(gate_weight, 'sp', axis=0, tiled=True)  61.7 us
    all_gather x1, waiting for transfers between devices, body(): lax.all_gather(value_weight, 'sp', axis=0, tiled=True)  61.6 us
    all_gather x1, waiting for transfers between devices, body(): lax.all_gather(down_weight, 'sp', axis=1, tiled=True)  57.8 us
    all_gather x1, waiting for transfers between devices, body(): gathered = lax.all_gather(paired, 'sp', axis=0, tiled=True)  31.7 us
    reduce_scatter x1, waiting for transfers between devices, body(): lax.psum_scatter(partial_sum, 'tp', scatter_dimension=0, tiled=True)  30 us
    reduce_scatter x1, waiting for transfers between devices, body(): lax.psum_scatter(jnp.dot(mixed, out_weight, preferred_element_type=jnp.fl...  28.8 us
    all_gather x1, waiting for transfers between devices, body(): lax.all_gather(normalize(state, norm_gain), 'tp', axis=0, tiled=True)  16.8 us
    another operation x2, other arithmetic  10.9 us
  transfers between devices with their start and end apart: 8, of which 8 were waited for; matrix products, arithmetic and copies ran while one was open for 2% of the time, Pallas kernels for 0%

commit v1 on v0

--- a/solution.py
+++ b/solution.py
@@ -64,7 +64,12 @@
     sp_count = lax.axis_size("sp")
     block = tok_dev * min(sp_count, max(1, 1024 // tok_dev))
     paired = jnp.concatenate([keys, values], axis=1)
-    gathered = lax.all_gather(paired, "sp", axis=0, tiled=True)
+    ring = [paired]
+    for hop in range(3):
+        ring.append(lax.ppermute(ring[-1], "sp", [(dev, (dev + 1) % 4) for dev in range(4)]))
+    gathered = jnp.roll(
+        jnp.concatenate(ring[::-1], axis=0), (lax.axis_index("sp") + 1) * ring[0].shape[0], axis=0
+    )
     mine = lax.axis_index("sp")
     query_place = mine * tok_dev + jnp.arange(tok_dev, dtype=jnp.int32)
     query_rows = queries.reshape(tok_dev, head_count, HEAD)

time: 384 us -> 351 us (0.914)
  waiting for transfers between devices: 292 us -> 253 us
    all_gather x1 -> x0, waiting for transfers between devices: 31.7 us -> none  [body(): gathered = lax.all_gather(paired, 'sp', axis=0, tiled=True)]
    all_gather x1, waiting for transfers between devices: 61.7 us -> 30.6 us  [body(): lax.all_gather(gate_weight, 'sp', axis=0, tiled=True)]
    ppermute x0 -> x3, waiting for transfers between devices: none -> 25 us  [body(): lax.ppermute(ring[-1], 'sp', [(dev, (dev + 1) % 4) for dev in range(4)])]
  transfers between devices with their start and end apart: 8 -> 10, of which waited for: 8 -> 10; matrix products, arithmetic and copies ran while one was open for 2% -> 3% of each run, Pallas kernels for 0% -> 0%
where the time goes in v1:
time: 351 us; the launch traced here: 350 us
  waiting for transfers between devices  253 us (72%)
  other arithmetic  26.3 us (7%)
  local copies, waits for them, and re-layouts  25.9 us (7%)
  matrix products  25.1 us (7%)
  between operations  15.3 us (4%)
  starting transfers between devices  4.61 us (1%)
    all_gather x1, waiting for transfers between devices, body(): lax.all_gather(value_weight, 'sp', axis=0, tiled=True)  61.5 us
    all_gather x1, waiting for transfers between devices, body(): lax.all_gather(down_weight, 'sp', axis=1, tiled=True)  57.9 us
    all_gather x1, waiting for transfers between devices, body(): lax.all_gather(gate_weight, 'sp', axis=0, tiled=True)  30.6 us
    reduce_scatter x1, waiting for transfers between devices, body(): lax.psum_scatter(partial_sum, 'tp', scatter_dimension=0, tiled=True)  30 us
    reduce_scatter x1, waiting for transfers between devices, body(): lax.psum_scatter(jnp.dot(mixed, out_weight, preferred_element_type=jnp.fl...  28.4 us
    ppermute x3, waiting for transfers between devices, body(): lax.ppermute(ring[-1], 'sp', [(dev, (dev + 1) % 4) for dev in range(4)])  25 us
    all_gather x1, waiting for transfers between devices, body(): lax.all_gather(normalize(state, norm_gain), 'tp', axis=0, tiled=True)  16.7 us
    another operation x2, other arithmetic  10.9 us
  transfers between devices with their start and end apart: 10, of which 10 were waited for; matrix products, arithmetic and copies ran while one was open for 3% of the time, Pallas kernels for 0%

profile of v1, /device:TPU:0, one launch (start us, length us, event | category | flops | bytes accessed | tf_op | source)
XLA Modules:
  0.0 350.2 jit_solution(15778537224083809191)
XLA Ops:
  7.4 1.1 copy.14
  8.5 1.0 copy.15
  9.5 3.1 collective-permute-start
  12.6 8.3 %collective-permute-done = bf16[256,512]{0,1:T(8,128)(2,1)S(1)} collective-permute-done((bf16[256,512]{0,1:T(8,128)(2,1)S(1)}, bf16[256,512]{0,1:T(8,128)(2,1)S(1)}, u32[]{:S(2)}, u32[]{:S(2)}) %collective-permute-start) | collective-permute-done | bytes 262176 | tf_op jit(solution)/shard_map/ppermute | solution.py:69
  20.9 9.3 %collective-permute-done.1 = bf16[256,512]{0,1:T(8,128)(2,1)S(1)} collective-permute-done((bf16[256,512]{0,1:T(8,128)(2,1)S(1)}, bf16[256,512]{0,1:T(8,128)(2,1)S(1)}, u32[]{:S(2)}, u32[]{:S(2)}) %collective-permute-start.1) | collective-permute-done | bytes 262176 | tf_op jit(solution)/shard_map/ppermute | solution.py:69
  30.2 1.0 copy.16
  31.2 7.4 %collective-permute-done.2 = bf16[256,512]{0,1:T(8,128)(2,1)S(1)} collective-permute-done((bf16[256,512]{0,1:T(8,128)(2,1)S(1)}, bf16[256,512]{0,1:T(8,128)(2,1)S(1)}, u32[]{:S(2)}, u32[]{:S(2)}) %collective-permute-start.2) | collective-permute-done | bytes 262176 | tf_op jit(solution)/shard_map/ppermute | solution.py:69
  38.9 0.1 constant_dynamic-slice_fusion
  39.0 0.7 broadcast_in_dim.23
  39.7 55.4 %while.11 = (s32[]{:T(128)}, f32[4,256,64]{1,2,0:T(8,128)}, s32[]{:T(128)}, bf16[1024,512]{0,1:T(8,128)(2,1)S(1)}, bf16[256,4,64]{0,2,1:T(8,128)(2,1)S(1)}, /*index=5*/s32[]{:T(128)}, s32[]{:T(128)}, s32[]{:T(128)}, f32[]{:T(128)}) while((s32[]{:T(128)}, f32[4,256,64]{1,2,0:T(8,128)}, s32[]{:T(128)}, ...), condition=%wide.region_4.5_spmd.clone, body=%wide.region_0.4_spmd.clone.sunk | while | flops 447937792 | bytes 95811784 | solution.py:87
  39.7 0.1 fusion.66
  39.8 2.9 fusion.67
  42.7 0.2 broadcast_compare_fusion.2
  43.0 5.6 %fusion.68 = (f32[4,256]{1,0:T(4,128)S(1)}, f32[4,256,1024]{2,1,0:T(8,128)S(1)}) fusion(f32[4,256,1024]{2,1,0:T(8,128)} %get-tuple-element.134, u8[256,1024]{1,0:T(8,128)(4,1)S(1)} %get-tuple-element.135, pred[256,1024]{1,0:T(8,128)(4,1)S(1)} %broadcast_compare_fusion.2), kind=kLoop, calls=%fused_computation.20.clone.1 | loop fusion | flops 13630464 | bytes 8916992 | tf_op jit(solution)/shard_map/while/body/reduce_sum | solution.py:27
  48.6 3.0 copy.21
  51.5 5.6 %copy.22 = f32[4,256,8,128]{1,2,3,0:T(8,128)} copy(f32[4,256,8,128]{3,2,1,0:T(8,128)} %bitcast.44) | data formatting | bytes 8388608 | tf_op jit(solution)/shard_map/reshape
  57.1 10.8 %fusion.69 = f32[4,256,8,128]{1,2,3,0:T(8,128)S(1)} fusion(f32[4,256,8,128]{1,2,3,0:T(8,128)} %copy.22), kind=kOutput, calls=%fused_computation.74.clone.1 | output fusion | flops 133169152 | bytes 8388608 | tf_op jit(solution)/shard_map/reduce-window
  67.9 2.0 copy-done.1
  69.9 0.1 reduce-window.16
  69.9 4.5 %broadcast_add_fusion.2 = f32[4,256,8,128]{1,2,3,0:T(8,128)} fusion(f32[4,256,8,128]{1,2,3,0:T(8,128)} %copy-done.1, f32[4,256,8]{1,2,0:T(8,128)S(1)} %slice.148), kind=kLoop, calls=%fused_computation.10.clone.1 | loop fusion | flops 1048576 | bytes 8421376 | tf_op jit(solution)/shard_map/reduce_window_sum | solution.py:22
  74.4 5.5 %copy.23 = f32[4,256,8,128]{3,2,1,0:T(8,128)} copy(f32[4,256,8,128]{1,2,3,0:T(8,128)} %broadcast_add_fusion.2) | data formatting | bytes 8388608 | tf_op jit(solution)/shard_map/reduce_window_sum | solution.py:22
  79.9 4.9 %reduce_window_sum.20 = f32[4,256,1024]{2,1,0:T(8,128)} reshape(f32[4,256,8,128]{3,2,1,0:T(8,128)} %copy.23) | data formatting | bytes 8388608 | tf_op jit(solution)/shard_map/reduce_window_sum | solution.py:22
  84.9 9.5 %fusion.70 = f32[4,256,64]{1,2,0:T(8,128)S(1)} fusion(bf16[1024,4,64]{0,2,1:T(8,128)(2,1)S(1)} %bitcast.46, f32[4,256,1024]{2,1,0:T(8,128)} %reduce_window_sum.20, f32[4,256,1024]{2,1,0:T(8,128)} %get-tuple-element.134, pred[256,1024]{1,0:T(8,128)(4,1)S(1)} %broadcast_compare_fusion.2, f32[4,256,64]{1,2,0:T(8,128)S(1)} %copy-done.2, ...), kind=kOutput, calls=%fused_computation.12.clone.1 | convolution fusion | flops 159514624 | bytes 9965568 | tf_op jit(solution)/shard_map/while/body/hqk,khe->hqe/dot_general | solution.py:26
  94.4 0.7 copy-done.3
  95.1 1.0 convert_element_type.44
  96.1 1.8 fusion.39
  98.0 0.0 all-gather.7.cloned.1.call-start
  98.0 0.5 all-gather.7.cloned.1.call-update
  98.6 0.0 all-gather.5.cloned.1.call-start
  98.6 28.4 %reduce-scatter.3.cloned.1.call-done = f32[64,2048]{1,0:T(8,128)} async-done(((f32[256,2048]{1,0:T(8,128)}), f32[64,2048]{1,0:T(8,128)}) %reduce-scatter.3.cloned.1.call-update) | async-done | bytes 524304 | tf_op jit(solution)/shard_map/reduce_scatter | solution.py:89
  127.1 1.2 fusion.22
  128.3 0.8 fusion.24
  129.2 0.0 all-gather.9.cloned.1.call-start
  129.2 0.5 all-gather.9.cloned.1.call-update
  129.8 0.7 all-gather.11.cloned.1.call-update
  130.5 30.6 %all-gather.7.cloned.1.call-done = bf16[2048,768]{1,0:T(8,128)(2,1)} async-done(((bf16[512,768]{1,0:T(8,128)(2,1)}), bf16[2048,768]{1,0:T(8,128)(2,1)}) %all-gather.7.cloned.1.call-update) | async-done | bytes 3145744 | tf_op jit(solution)/shard_map/all_gather | solution.py:100
  161.2 16.7 %all-gather.5.cloned.1.call-done = bf16[256,2048]{1,0:T(8,128)(2,1)} async-done(((bf16[64,2048]{1,0:T(8,128)(2,1)}), bf16[256,2048]{1,0:T(8,128)(2,1)}) %all-gather.5.cloned.1.call-update) | async-done | bytes 1048592 | tf_op jit(solution)/shard_map/all_gather | solution.py:96
  177.8 3.3 convolution_convert_fusion.1
  181.1 61.5 %all-gather.9.cloned.1.call-done = bf16[2048,768]{1,0:T(8,128)(2,1)} async-done(((bf16[512,768]{1,0:T(8,128)(2,1)}), bf16[2048,768]{1,0:T(8,128)(2,1)}) %all-gather.9.cloned.1.call-update) | async-done | bytes 3145744 | tf_op jit(solution)/shard_map/all_gather | solution.py:105
  242.6 2.9 convolution_convert_fusion
  245.5 1.3 collective-permute-start.3
  246.8 0.1 slice_reduce_fusion.2
  246.9 1.2 collective-permute-done.3
  248.1 0.2 maximum_convert_fusion
  248.3 57.9 %all-gather.11.cloned.1.call-done = bf16[768,2048]{1,0:T(8,128)(2,1)} async-done(((bf16[768,512]{1,0:T(8,128)(2,1)}), bf16[768,2048]{1,0:T(8,128)(2,1)}) %all-gather.11.cloned.1.call-update) | async-done | bytes 3145744 | tf_op jit(solution)/shard_map/all_gather | solution.py:120
  306.2 4.7 %fusion.26 = f32[256,2048]{1,0:T(8,128)} fusion(bf16[768,2048]{1,0:T(8,128)(2,1)} %all-gather.11.cloned.1.call-done, f32[258,768]{1,0:T(8,128)S(1)} %get-tuple-element.84, f32[258,768]{1,0:T(8,128)S(1)} %get-tuple-element.83, f32[768]{0:T(1024)S(1)} %get-tuple-element.59, f32[768]{0:T(1024)S(1)} %get-tuple-element.60, f32[768]{0:T(1024)S(1)} %get-tuple-element.58, ...), kind=kOutput, calls=%fused_computation.45 | convolution fusion | flops 808452096 | bytes 9986048 | tf_op jit(solution)/shard_map/dot_general | solution.py:118
  310.9 30.0 %reduce-scatter.5.cloned.1.call-done = f32[64,2048]{1,0:T(8,128)} async-done(((f32[256,2048]{1,0:T(8,128)}), f32[64,2048]{1,0:T(8,128)}) %reduce-scatter.5.cloned.1.call-update) | async-done | bytes 524304 | tf_op jit(solution)/shard_map/reduce_scatter | solution.py:123
  340.8 1.8 fusion.25
  (43 shorter events, 0.5 us)
Async XLA Ops:
  7.4 88.8 %copy-start = (bf16[256,2048]{1,0:T(8,128)(2,1)S(1)}, bf16[256,2048]{1,0:T(8,128)(2,1)}, u32[]{:S(2)}) copy-start(bf16[256,2048]{1,0:T(8,128)(2,1)} %param.17) | copy-start | bytes 3145732
  7.4 119.7 %reduce-scatter.3.cloned.1.call-start = ((), (), s32[]{:S(2)}) async-start(), calls=%async_computation.2 | async-start | bytes 2621440 | tf_op jit(solution)/shard_map/reduce_scatter | solution.py:89
  9.5 11.4 %collective-permute-start = (bf16[256,512]{0,1:T(8,128)(2,1)S(1)}, bf16[256,512]{0,1:T(8,128)(2,1)S(1)}, u32[]{:S(2)}, u32[]{:S(2)}) collective-permute-start(bf16[256,512]{0,1:T(8,128)(2,1)S(1)} %pad_maximum_fusion), channel_id=1, source_target_pairs={{0,4},{4,8},{8,12},{12,0},{1,5},{5,9},{9,13},{13,1},{2,6},{6,10},{... | collective-permute-start | bytes 786440 | tf_op jit(solution)/shard_map/ppermute | solution.py:69
  20.9 9.3 %collective-permute-start.1 = (bf16[256,512]{0,1:T(8,128)(2,1)S(1)}, bf16[256,512]{0,1:T(8,128)(2,1)S(1)}, u32[]{:S(2)}, u32[]{:S(2)}) collective-permute-start(bf16[256,512]{0,1:T(8,128)(2,1)S(1)} %collective-permute-done), channel_id=1, source_target_pairs={{0,4},{4,8},{8,12},{12,0},{1,5},{5,9},{9,13},{13,1},{2,6},{6,10},{... | collective-permute-start | bytes 786440 | tf_op jit(solution)/shard_map/ppermute | solution.py:69
  30.2 8.4 %collective-permute-start.2 = (bf16[256,512]{0,1:T(8,128)(2,1)S(1)}, bf16[256,512]{0,1:T(8,128)(2,1)S(1)}, u32[]{:S(2)}, u32[]{:S(2)}) collective-permute-start(bf16[256,512]{0,1:T(8,128)(2,1)S(1)} %collective-permute-done.1), channel_id=1, source_target_pairs={{0,4},{4,8},{8,12},{12,0},{1,5},{5,9},{9,13},{13,1},{2,6},{6,10},{... | collective-permute-start | bytes 786440 | tf_op jit(solution)/shard_map/ppermute | solution.py:69
  67.9 2.0 copy-start.1
  79.9 5.0 %copy-start.2 = (f32[4,256,64]{1,2,0:T(8,128)S(1)}, f32[4,256,64]{1,2,0:T(8,128)}, u32[]{:S(2)}) copy-start(f32[4,256,64]{1,2,0:T(8,128)} %get-tuple-element.148) | copy-start | bytes 786436 | tf_op jit(solution)/shard_map/while
  94.4 0.7 copy-start.3
  95.1 31.9 %copy-start.4 = (bf16[64,2048]{1,0:T(8,128)(2,1)S(1)}, bf16[64,2048]{1,0:T(8,128)(2,1)}, u32[]{:S(2)}) copy-start(bf16[64,2048]{1,0:T(8,128)(2,1)} %param.16) | copy-start | bytes 786436
  95.1 33.2 %copy-start.5 = (f32[2048]{0:T(1024)S(1)}, f32[2048]{0:T(1024)}, u32[]{:S(2)}) copy-start(f32[2048]{0:T(1024)} %param.22) | copy-start | bytes 24580
  98.0 63.2 %all-gather.7.cloned.1.call-start = ((), (), s32[]{:S(2)}) async-start(), calls=%async_computation.4 | async-start | bytes 3932160 | tf_op jit(solution)/shard_map/all_gather | solution.py:100
  98.6 79.2 %all-gather.5.cloned.1.call-start = ((), (), s32[]{:S(2)}) async-start(), calls=%async_computation.3 | async-start | bytes 1310720 | tf_op jit(solution)/shard_map/all_gather | solution.py:96
  129.2 113.4 %all-gather.9.cloned.1.call-start = ((), (), s32[]{:S(2)}) async-start(), calls=%async_computation.5 | async-start | bytes 3932160 | tf_op jit(solution)/shard_map/all_gather | solution.py:105
  129.8 176.4 %all-gather.11.cloned.1.call-start = ((), (), s32[]{:S(2)}) async-start(), calls=%async_computation.6 | async-start | bytes 3932160 | tf_op jit(solution)/shard_map/all_gather | solution.py:120
  130.5 210.3 %reduce-scatter.5.cloned.1.call-start = ((), (), s32[]{:S(2)}) async-start(), calls=%async_computation.7 | async-start | bytes 2621440 | tf_op jit(solution)/shard_map/reduce_scatter | solution.py:123
  177.8 64.8 %copy-start.8 = (bf16[256,2048]{1,0:T(8,128)(2,1)S(1)}, bf16[256,2048]{1,0:T(8,128)(2,1)}, u32[]{:S(2)}) copy-start(bf16[256,2048]{1,0:T(8,128)(2,1)} %all-gather.5.cloned.1.call-done) | copy-start | bytes 3145732
  181.1 65.7 %copy-start.6 = (f32[3,768]{1,0:T(4,128)S(1)}, f32[3,768]{1,0:T(4,128)}, u32[]{:S(2)}) copy-start(f32[3,768]{1,0:T(4,128)} %param.21) | copy-start | bytes 27652
  181.1 65.7 %copy-start.7 = (f32[3,768]{1,0:T(4,128)S(1)}, f32[3,768]{1,0:T(4,128)}, u32[]{:S(2)}) copy-start(f32[3,768]{1,0:T(4,128)} %param.20) | copy-start | bytes 27652
  245.5 2.6 collective-permute-start.3
Sparse Core Ops, SparseCore 0:
  98.1 28.8 reduce-scatter.2
  311.0 29.7 reduce-scatter.4
Sparse Core Ops, SparseCore 1:
  100.0 61.0 all-gather.6
  162.6 15.2 all-gather.4
  179.3 63.3 all-gather.8
  244.2 61.9 all-gather.10
